TPU v7x, 128 devices: a whole 4x4x4 slice. The times are simulated.
128 devices in a mesh: ep: 32 (over z, y, core), tp: 4 (over x).
Axes of the slice: x: 4, y: 4, z: 4, core: 2. Of those that a mesh axis runs over, the one named last changes fastest.
Arguments:
- q_latent: bfloat16 [16384, 512], P(('ep', 'tp')), may hold values from -6 to 6
- kv_latent: bfloat16 [16384, 256], P(('ep', 'tp')), may hold values from -6 to 6
- rope_key: bfloat16 [16384, 32], P(('ep', 'tp')), may hold values from -240 to 240
- q_gain: float32 [512], replicated, may hold values from 0.1 to 1.9
- kv_gain: float32 [256], replicated, may hold values from 0.1 to 1.9
- w_query: bfloat16 [512, 1024], P(None, 'tp'), may hold values from -0.25 to 0.25
- w_query_rot: bfloat16 [512, 512], P(None, 'tp'), may hold values from -0.25 to 0.25
- w_key: bfloat16 [256, 1024], P(None, 'tp'), may hold values from -0.375 to 0.375
- w_value: bfloat16 [256, 1024], P(None, 'tp'), may hold values from -0.375 to 0.375
- w_mix_out: bfloat16 [1024, 2048], P('tp'), may hold values from -0.1875 to 0.1875
- expert_input: bfloat16 [16384, 2048], P(('ep', 'tp')), may hold values from -6 to 6
- ffn_gain: float32 [2048], replicated, may hold values from 0.1 to 1.9
- expert_ids: int32 [16384, 4], P(('ep', 'tp')), may hold values from 0 to 31, all different within a row; in each aligned block of 128 rows (0 to 127, 128 to 255, ...) at most 24 rows name the same one
- route_weights: float32 [16384, 4], P(('ep', 'tp')), may hold values from 0.2 to 1
- w_gate_exp: bfloat16 [32, 2048, 1024], P('ep', None, 'tp'), may hold values from -0.125 to 0.125
- w_up_exp: bfloat16 [32, 2048, 1024], P('ep', None, 'tp'), may hold values from -0.125 to 0.125
- w_down_exp: bfloat16 [32, 1024, 2048], P('ep', 'tp'), may hold values from -0.1875 to 0.1875
Outputs:
- mixer_out: bfloat16 [16384, 2048], P(('ep', 'tp'))
- expert_out: bfloat16 [16384, 2048], P(('ep', 'tp'))
Inputs may be any that keep to these rules, and one draw needn't show every extreme that they name: `expert_ids`: the experts of a row are all different. In the rows of one device (aligned blocks of 128 tokens) no expert is named by more than 24 rows, a bound that some block reaches.
All inputs are finite; a program needn't handle non-finite values.
Results may differ from a plain program's by a relative error of at most 0.012.
The roundings to bfloat16 on the way count: a program that leaves them out, or rounds other values in their place, can miss the bound.
Values may be sent and summed in bfloat16 or wider, within the bound.
A program may use at most 128 MiB of HBM per device.

v0:
```python
import jax
import jax.numpy as jnp
from jax import lax
from jax.sharding import PartitionSpec as P

D = 2048
NOPE = 64
ROPE = 32
VD = 64
TOPK = 4
SEG = 64
norm_epsilon = 1e-06
rope_base = 10000.0
masked_score = -1e30


def rms_scale(values_in, gain_vec):
    floats = values_in.astype(jnp.float32)
    return (
        floats
        * lax.rsqrt(jnp.mean(floats * floats, axis=-1, keepdims=True) + norm_epsilon)
        * gain_vec
    )


def tables(positions):
    half_width = ROPE // 2
    frequency = rope_base ** (-jnp.arange(half_width, dtype=jnp.float32) / half_width)
    angles = positions.astype(jnp.float32)[:, None] * frequency[None, :]
    return (jnp.cos(angles), jnp.sin(angles))


def rotate_pairs(values_in, cosine, sine_table):
    half_width = values_in.shape[-1] // 2
    first, second = (values_in[..., :half_width], values_in[..., half_width:])
    return jnp.concatenate(
        [first * cosine - second * sine_table, first * sine_table + second * cosine], axis=-1
    )


def on_device(
    q_latent,
    kv_latent,
    rope_key,
    q_gain,
    kv_gain,
    w_query,
    w_query_rot,
    w_key,
    w_value,
    w_mix_out,
    expert_input,
    ffn_gain,
    expert_ids,
    route_weights,
    w_gate_exp,
    w_up_exp,
    w_down_exp,
):
    tok_rows = q_latent.shape[0]
    tp_count = lax.axis_size("tp")
    group_rows = tp_count * tok_rows
    group_start = lax.axis_index("ep") * group_rows
    heads_here = w_key.shape[1] // NOPE
    score_scale = (NOPE + ROPE) ** (-0.5)
    shard_rows = lax.all_gather(q_latent, "tp", axis=0, tiled=True)
    row_count = shard_rows.shape[0]
    positions = group_start + jnp.arange(row_count, dtype=jnp.int32)
    cosine, sine_table = tables(positions)
    normed = rms_scale(shard_rows, q_gain).astype(jnp.bfloat16)
    plain = jnp.dot(normed, w_query, preferred_element_type=jnp.float32).astype(jnp.bfloat16)
    turned = jnp.dot(normed, w_query_rot, preferred_element_type=jnp.float32).reshape(
        row_count, heads_here, ROPE
    )
    turned = rotate_pairs(turned, cosine[:, None, :], sine_table[:, None, :]).astype(jnp.bfloat16)
    queries = jnp.concatenate([plain, turned.reshape(row_count, heads_here * ROPE)], axis=1)
    q_plain = queries[:, : heads_here * NOPE].reshape(group_rows, heads_here, NOPE)
    q_turned = queries[:, heads_here * NOPE :].reshape(group_rows, heads_here, ROPE)
    query_segment = (group_start + jnp.arange(group_rows, dtype=jnp.int32)) // SEG
    last_segment = (group_start + group_rows - 1) // SEG
    start_state = (
        jnp.full((heads_here, group_rows), masked_score, jnp.float32),
        jnp.zeros((heads_here, group_rows), jnp.float32),
        jnp.zeros((heads_here, group_rows, VD), jnp.float32),
    )
    first_row = jnp.int32(0)
    latents = lax.all_gather(kv_latent, ("ep", "tp"), axis=0, tiled=True)
    rope_rows = lax.all_gather(rope_key, ("ep", "tp"), axis=0, tiled=True)
    shard_count = latents.shape[0] // tok_rows
    grouping = 1
    for divisor in range(1, shard_count + 1):
        if shard_count % divisor == 0 and divisor * tok_rows <= max(512, tok_rows):
            grouping = divisor
    key_rows = grouping * tok_rows

    def key_work(state, offset):
        run_max, weight_sum, weighted = state
        latent_block = lax.dynamic_slice_in_dim(latents, offset, key_rows, 0)
        rope_block = lax.dynamic_slice_in_dim(rope_rows, offset, key_rows, 0)
        positions = first_row + offset + jnp.arange(key_rows, dtype=jnp.int32)
        cosine, sine_table = tables(positions)
        normed = rms_scale(latent_block, kv_gain).astype(jnp.bfloat16)
        k_plain = jnp.dot(normed, w_key, preferred_element_type=jnp.float32).astype(jnp.bfloat16)
        k_plain = k_plain.reshape(key_rows, heads_here, NOPE)
        values = jnp.dot(normed, w_value, preferred_element_type=jnp.float32).astype(jnp.bfloat16)
        values = values.reshape(key_rows, heads_here, VD)
        k_turned = rotate_pairs(rope_block.astype(jnp.float32), cosine, sine_table).astype(
            jnp.bfloat16
        )
        scores = jnp.einsum("qhd,khd->hqk", q_plain, k_plain, preferred_element_type=jnp.float32)
        scores = scores + jnp.einsum(
            "qhd,kd->hqk", q_turned, k_turned, preferred_element_type=jnp.float32
        )
        scores = scores * score_scale
        allowed = (positions // SEG)[None, :] <= query_segment[:, None]
        scores = jnp.where(allowed[None], scores, masked_score)
        new_max = jnp.maximum(run_max, jnp.max(scores, axis=-1))
        weights = jnp.where(allowed[None], jnp.exp(scores - new_max[:, :, None]), 0.0)
        factor = jnp.exp(run_max - new_max)
        weight_sum = weight_sum * factor + jnp.sum(weights, axis=-1)
        weighted = weighted * factor[:, :, None] + jnp.einsum(
            "hqk,khd->hqd", weights.astype(jnp.bfloat16), values, preferred_element_type=jnp.float32
        )
        return (new_max, weight_sum, weighted)

    def key_step(state, block_number):
        offset = block_number * key_rows
        visible = (first_row + offset) // SEG <= last_segment
        updated = lax.cond(
            visible, lambda carried: key_work(carried, offset), lambda carried: carried, state
        )
        return (updated, None)

    result_state, _ = lax.scan(
        key_step, start_state, jnp.arange(shard_count // grouping, dtype=jnp.int32)
    )
    run_max, weight_sum, weighted = result_state
    attention = (
        (weighted / weight_sum[:, :, None])
        .transpose(1, 0, 2)
        .astype(jnp.bfloat16)
        .reshape(group_rows, heads_here * VD)
    )
    chosen = attention
    partial_out = jnp.dot(chosen, w_mix_out, preferred_element_type=jnp.float32).astype(
        jnp.bfloat16
    )
    mixer_out = lax.psum_scatter(
        lax.optimization_barrier(partial_out).astype(jnp.float32).astype(jnp.bfloat16),
        "tp",
        scatter_dimension=0,
        tiled=True,
    )
    expert_count = lax.axis_size("ep")
    slot_count = 3 * tok_rows * TOPK // (2 * expert_count)
    gate_weight = w_gate_exp[0]
    up_weight = w_up_exp[0]
    down_weight = w_down_exp[0]
    normed = rms_scale(expert_input, ffn_gain).astype(jnp.bfloat16)
    routed = expert_ids.reshape(-1)
    onehot = (routed[:, None] == jnp.arange(expert_count, dtype=jnp.int32)[None, :]).astype(
        jnp.int32
    )
    slot_number = jnp.sum((jnp.cumsum(onehot, axis=0) - 1) * onehot, axis=-1)
    slot_place = (routed * slot_count + slot_number).reshape(tok_rows, TOPK)
    slot_line = jnp.arange(expert_count * slot_count, dtype=jnp.int32)
    picks = [
        (slot_place[:, route_rank][:, None] == slot_line[None, :]).astype(jnp.bfloat16)
        for route_rank in range(TOPK)
    ]
    dispatch = picks[0]
    for route_rank in range(1, TOPK):
        dispatch = dispatch + picks[route_rank]
    outgoing = lax.dot_general(
        dispatch, normed, (((0,), (0,)), ((), ())), preferred_element_type=jnp.float32
    ).astype(jnp.bfloat16)
    copies = jnp.broadcast_to(
        outgoing.reshape(expert_count, 1, slot_count, D), (expert_count, tp_count, slot_count, D)
    )
    copies = copies.reshape(expert_count * tp_count, slot_count, D)
    arrived = lax.all_to_all(copies, ("ep", "tp"), split_axis=0, concat_axis=0, tiled=True)
    sources, item_count, feature_width = arrived.shape
    chosen = arrived.reshape(sources * item_count, feature_width)
    gate_part = jnp.dot(chosen, gate_weight, preferred_element_type=jnp.float32)
    up_part = jnp.dot(chosen, up_weight, preferred_element_type=jnp.float32)
    hidden = (jax.nn.silu(gate_part) * up_part).astype(jnp.bfloat16)
    partial_out = jnp.dot(hidden, down_weight, preferred_element_type=jnp.float32).astype(
        jnp.bfloat16
    )
    returned = lax.all_to_all(
        partial_out.reshape(sources, item_count, feature_width),
        ("ep", "tp"),
        split_axis=0,
        concat_axis=0,
        tiled=True,
    )
    block_parts = returned.reshape(expert_count, tp_count, slot_count, D).astype(jnp.float32)
    results = (
        jnp.sum(block_parts, axis=1).astype(jnp.bfloat16).reshape(expert_count * slot_count, D)
    )
    combined = jnp.zeros((tok_rows, D), jnp.float32)
    for route_rank in range(TOPK):
        fetched = jnp.dot(picks[route_rank], results, preferred_element_type=jnp.float32)
        combined = combined + route_weights[:, route_rank : route_rank + 1] * fetched
    expert_out = combined.astype(jnp.bfloat16)
    return (mixer_out, expert_out)


def solution(mesh):
    return jax.shard_map(
        on_device,
        mesh=mesh,
        in_specs=(
            P(("ep", "tp"), None),
            P(("ep", "tp"), None),
            P(("ep", "tp"), None),
            P(),
            P(),
            P(None, "tp"),
            P(None, "tp"),
            P(None, "tp"),
            P(None, "tp"),
            P("tp", None),
            P(("ep", "tp"), None),
            P(),
            P(("ep", "tp"), None),
            P(("ep", "tp"), None),
            P("ep", None, "tp"),
            P("ep", None, "tp"),
            P("ep", "tp", None),
        ),
        out_specs=(P(("ep", "tp"), None), P(("ep", "tp"), None)),
        check_vma=False,
    )
```

profile of v0, /device:TPU:1, one launch (start us, length us, event | category | flops | bytes accessed | tf_op | source)
XLA Modules:
  0.0 609.9 jit_solution(8935028124554305752)
XLA Ops:
  7.2 0.7 all-gather.5.cloned.1.call-update
  8.0 0.7 all-gather.3.cloned.1.call-update
  8.7 0.8 copy.33
  9.7 1.2 reduce-window.6
  11.4 0.7 multiply_add_fusion.1
  12.1 1.2 fusion.50
  13.4 3.9 convolution_convert_fusion.3
  17.3 8.2 %broadcast_in_dim.42 = bf16[32,4,24,2048]{3,2,1,0:T(8,128)(2,1)} broadcast(bf16[32,24,2048]{2,1,0:T(8,128)(2,1)} %bitcast.95), dimensions={0,2,3} | broadcast | bytes 15728640 | tf_op jit(solution)/shard_map/broadcast_in_dim | solution.py:177
  25.5 11.9 %all-to-all-start = ((bf16[128,24,2048]{2,1,0:T(8,128)(2,1)}), bf16[128,24,2048]{2,1,0:T(8,128)(2,1)}, u32[]{:S(2)}, u32[]{:S(2)}) async-start(bf16[128,24,2048]{2,1,0:T(8,128)(2,1)} %bitcast.91), calls=%async_computation.1 | async-start | bytes 25165824 | tf_op jit(solution)/shard_map/all_to_all | solution.py:181
  37.4 156.9 %all_gather.10 = bf16[512,512]{1,0:T(8,128)(2,1)S(1)} all-gather(bf16[128,512]{1,0:T(8,128)(2,1)S(1)} %copy-done.6), channel_id=1, replica_groups=mesh['ep'=32,'tp'=4] {'tp'}, dimensions={0}, use_global_device_ids=true | all-gather | bytes 655360 | tf_op jit(solution)/shard_map/all_gather | solution.py:66
  195.7 1.2 all-to-all-done
  196.9 9.7 %fusion.56 = f32[3072,256]{1,0:T(8,128)} fusion(bf16[3072,2048]{1,0:T(8,128)(2,1)} %bitcast.17, bf16[1,2048,256]{2,1,0:T(8,128)(2,1)S(1)} %copy-done.9), kind=kOutput, calls=%fused_computation.90 | convolution fusion | flops 3221225472 | bytes 16777216 | tf_op jit(solution)/shard_map/dot_general | solution.py:184
  206.5 19.1 %convolution_convert_fusion.2 = bf16[3072,2048]{1,0:T(8,128)(2,1)} fusion(bf16[3072,2048]{1,0:T(8,128)(2,1)} %bitcast.17, f32[3072,256]{1,0:T(8,128)} %fusion.56, bf16[1,256,2048]{2,1,0:T(8,128)(2,1)S(1)} %copy-done, bf16[1,2048,256]{2,1,0:T(8,128)(2,1)} %param.36), kind=kOutput, calls=%fused_computation.63 | convolution fusion | flops 6453460992 | bytes 30408704 | tf_op jit(solution)/shard_map/dot_general | solution.py:187
  225.6 15.1 %all-to-all-start.1 = ((bf16[128,24,2048]{2,1,0:T(8,128)(2,1)}), bf16[128,24,2048]{2,1,0:T(8,128)(2,1)}, u32[]{:S(2)}, u32[]{:S(2)}) async-start(bf16[128,24,2048]{2,1,0:T(8,128)(2,1)} %bitcast.94), calls=%async_computation.2 | async-start | bytes 25165824 | tf_op jit(solution)/shard_map/all_to_all | solution.py:190
  241.1 17.0 %all-gather.3.cloned.1.call-done = bf16[16384,256]{1,0:T(8,128)(2,1)} async-done(((bf16[128,256]{1,0:T(8,128)(2,1)}), bf16[16384,256]{1,0:T(8,128)(2,1)}) %all-gather.3.cloned.1.call-update) | async-done | bytes 8388624 | tf_op jit(solution)/shard_map/all_gather | solution.py:87
  258.2 57.2 %while.17 = (s32[]{:T(128)}, f32[4,512]{1,0:T(4,128)S(1)}, f32[4,512]{1,0:T(4,128)S(1)}, f32[4,512,64]{1,2,0:T(8,128)S(1)}, s32[32]{0:T(128)S(1)}, /*index=5*/s3...) while((s32[]{:T(128)}, f32[4,512]{1,0:T(4,128)S(1)}, ...), condition=%wide.region_7.8_spmd.clone, body=%wide.region_1.7_spmd.clone.sunk | while | flops 482656832 | bytes 25966364 | solution.py:134
  259.4 9.0 %conditional.3 = ((f32[4,512]{1,0:T(4,128)S(1)}, f32[4,512]{1,0:T(4,128)S(1)}, f32[4,512,64]{1,2,0:T(8,128)S(1)})) conditional(s32[]{:T(128)} %convert_element_type.193, (f32[4,512]{1,0:T(4,128)S(1)}, f32[4,512]{1,0:T(4,128)S(1)}, f32[4,512,64]{1,2,0:T(8,128)S(1)}) %tuple.59, (s32[]{:T(128)}, s32[512]{0:T(512)S(1)}, bf16[16384,256]{1,0:T(8,128)(2,1)}, ...), branch_computations={%region_2.2_spmd, %region_3.6_spmd} | conditional | flops 482649632 | bytes 25957090 | solution.py:129
  259.4 1.1 fusion.14
  260.6 1.3 convolution_convert_fusion.1
  261.9 0.8 fusion.88
  262.6 0.9 dynamic-slice_convert_fusion
  264.0 1.2 fusion.87
  265.2 0.8 fusion.5
  266.0 1.3 convolution_convert_fusion
  267.3 1.0 fusion.11
  268.4 0.6 dynamic_slice.20
  269.6 9.0 %conditional.3 = ((f32[4,512]{1,0:T(4,128)S(1)}, f32[4,512]{1,0:T(4,128)S(1)}, f32[4,512,64]{1,2,0:T(8,128)S(1)})) conditional(s32[]{:T(128)} %convert_element_type.193, (f32[4,512]{1,0:T(4,128)S(1)}, f32[4,512]{1,0:T(4,128)S(1)}, f32[4,512,64]{1,2,0:T(8,128)S(1)}) %tuple.59, (s32[]{:T(128)}, s32[512]{0:T(512)S(1)}, bf16[16384,256]{1,0:T(8,128)(2,1)}, ...), branch_computations={%region_2.2_spmd, %region_3.6_spmd} | conditional | flops 482649632 | bytes 25957090 | solution.py:129
  269.6 1.1 fusion.14
  270.7 1.3 convolution_convert_fusion.1
  272.1 0.8 fusion.88
  272.8 0.9 dynamic-slice_convert_fusion
  274.2 1.2 fusion.87
  275.4 0.8 fusion.5
  276.2 1.3 convolution_convert_fusion
  277.5 1.0 fusion.11
  281.0 0.6 dynamic_slice.20
  282.3 0.6 dynamic_slice.20
  285.9 0.6 dynamic_slice.20
  289.6 0.6 dynamic_slice.20
  293.3 0.6 dynamic_slice.20
  315.5 2.1 convolution_convert_fusion.4
  317.7 84.1 %all-to-all-done.1 = bf16[128,24,2048]{2,1,0:T(8,128)(2,1)} async-done(((bf16[128,24,2048]{2,1,0:T(8,128)(2,1)}), bf16[128,24,2048]{2,1,0:T(8,128)(2,1)}, u32[]{:S(2)}, u32[]{:S(2)}) %all-to-all-start.1) | async-done | bytes 12582944 | tf_op jit(solution)/shard_map/all_to_all | solution.py:190
  401.8 10.4 %bitcast_reduce_fusion = bf16[32,24,2048]{2,1,0:T(8,128)(2,1)} fusion(bf16[128,24,2048]{2,1,0:T(8,128)(2,1)} %all-to-all-done.1), kind=kLoop, calls=%fused_computation.62 | loop fusion | flops 4718592 | bytes 15728640 | tf_op jit(solution)/shard_map/reduce_sum | solution.py:199
  412.1 2.7 convolution_multiply_fusion.2
  415.0 0.6 convolution_multiply_fusion.3
  415.6 0.7 convolution_multiply_fusion.1
  416.3 1.6 fusion.45
  417.9 185.5 %reduce-scatter.2.cloned.1.call-done = bf16[128,2048]{1,0:T(8,128)(2,1)} async-done(((bf16[512,2048]{1,0:T(8,128)(2,1)}), bf16[128,2048]{1,0:T(8,128)(2,1)}) %reduce-scatter.2.cloned.1.call-update) | async-done | bytes 524304 | tf_op jit(solution)/shard_map/reduce_scatter | solution.py:148
  (259 shorter events, 19.6 us)
Async XLA Ops:
  7.2 199.4 %copy-start = (bf16[1,256,2048]{2,1,0:T(8,128)(2,1)S(1)}, bf16[1,256,2048]{2,1,0:T(8,128)(2,1)}, u32[]{:S(2)}) copy-start(bf16[1,256,2048]{2,1,0:T(8,128)(2,1)} %param.37) | copy-start | bytes 3145732
  7.2 233.9 %all-gather.5.cloned.1.call-start = ((), (), s32[]{:S(2)}) async-start(), calls=%async_computation.4 | async-start | bytes 1056768 | tf_op jit(solution)/shard_map/all_gather | solution.py:88
  7.9 250.1 %all-gather.3.cloned.1.call-start = ((), (), s32[]{:S(2)}) async-start(), calls=%async_computation.3 | async-start | bytes 8454144 | tf_op jit(solution)/shard_map/all_gather | solution.py:87
  25.5 12.0 %copy-start.6 = (bf16[128,512]{1,0:T(8,128)(2,1)S(1)}, bf16[128,512]{1,0:T(8,128)(2,1)}, u32[]{:S(2)}) copy-start(bf16[128,512]{1,0:T(8,128)(2,1)} %param.21) | copy-start | bytes 393220
  25.5 169.2 %copy-start.11 = (bf16[512,128]{1,0:T(8,128)(2,1)S(1)}, bf16[512,128]{1,0:T(8,128)(2,1)}, u32[]{:S(2)}) copy-start(bf16[512,128]{1,0:T(8,128)(2,1)} %param.27) | copy-start | bytes 393220
  25.5 169.2 %copy-start.12 = (f32[512]{0:T(512)S(1)}, f32[512]{0:T(512)}, u32[]{:S(2)}) copy-start(f32[512]{0:T(512)} %param.24) | copy-start | bytes 6148
  25.5 169.7 %copy-start.10 = (bf16[512,256]{1,0:T(8,128)(2,1)S(1)}, bf16[512,256]{1,0:T(8,128)(2,1)}, u32[]{:S(2)}) copy-start(bf16[512,256]{1,0:T(8,128)(2,1)} %param.26) | copy-start | bytes 786436
  25.5 171.4 %all-to-all-start = ((bf16[128,24,2048]{2,1,0:T(8,128)(2,1)}), bf16[128,24,2048]{2,1,0:T(8,128)(2,1)}, u32[]{:S(2)}, u32[]{:S(2)}) async-start(bf16[128,24,2048]{2,1,0:T(8,128)(2,1)} %bitcast.91), calls=%async_computation.1 | async-start | bytes 25165824 | tf_op jit(solution)/shard_map/all_to_all | solution.py:181
  37.4 159.5 %copy-start.9 = (bf16[1,2048,256]{2,1,0:T(8,128)(2,1)S(1)}, bf16[1,2048,256]{2,1,0:T(8,128)(2,1)}, u32[]{:S(2)}) copy-start(bf16[1,2048,256]{2,1,0:T(8,128)(2,1)} %param.35) | copy-start | bytes 3145732
  225.6 32.5 %copy-start.3 = (bf16[256,256]{1,0:T(8,128)(2,1)S(1)}, bf16[256,256]{1,0:T(8,128)(2,1)}, u32[]{:S(2)}) copy-start(bf16[256,256]{1,0:T(8,128)(2,1)} %param.28) | copy-start | bytes 393220
  225.6 32.5 %copy-start.4 = (bf16[256,256]{1,0:T(8,128)(2,1)S(1)}, bf16[256,256]{1,0:T(8,128)(2,1)}, u32[]{:S(2)}) copy-start(bf16[256,256]{1,0:T(8,128)(2,1)} %param.29) | copy-start | bytes 393220
  225.6 32.5 %copy-start.7 = (f32[256]{0:T(256)S(1)}, f32[256]{0:T(256)}, u32[]{:S(2)}) copy-start(f32[256]{0:T(256)} %param.25) | copy-start | bytes 3076
  225.6 176.1 %all-to-all-start.1 = ((bf16[128,24,2048]{2,1,0:T(8,128)(2,1)}), bf16[128,24,2048]{2,1,0:T(8,128)(2,1)}, u32[]{:S(2)}, u32[]{:S(2)}) async-start(bf16[128,24,2048]{2,1,0:T(8,128)(2,1)} %bitcast.94), calls=%async_computation.2 | async-start | bytes 25165824 | tf_op jit(solution)/shard_map/all_to_all | solution.py:190
  240.8 362.6 %reduce-scatter.2.cloned.1.call-start = ((), (), s32[]{:S(2)}) async-start(), calls=%async_computation.5 | async-start | bytes 2621440 | tf_op jit(solution)/shard_map/reduce_scatter | solution.py:148
  258.2 57.3 %copy-start.5 = (bf16[256,2048]{1,0:T(8,128)(2,1)S(1)}, bf16[256,2048]{1,0:T(8,128)(2,1)}, u32[]{:S(2)}) copy-start(bf16[256,2048]{1,0:T(8,128)(2,1)} %param.30) | copy-start | bytes 3145732
  315.4 2.2 copy-start.8
  412.1 2.8 copy-start.2
  415.6 187.8 %copy-start.1 = (bf16[1,256,2048]{2,1,0:T(8,128)(2,1)S(1)}, bf16[1,256,2048]{2,1,0:T(8,128)(2,1)}, u32[]{:S(2)}) copy-start(bf16[1,256,2048]{2,1,0:T(8,128)(2,1)} %param.37) | copy-start | bytes 3145732
Sparse Core Ops, SparseCore 0:
  10.8 144.9 all-gather.4
  159.0 99.0 all-gather.2
  317.8 285.5 reduce-scatter.1
where the time goes:
time: 616 us; the launch traced here: 610 us
  waiting for transfers between devices  289 us (47%)
  blocking collectives  157 us (25%)
  matrix products  52.5 us (9%)
  local copies, waits for them, and re-layouts  27.9 us (5%)
  starting transfers between devices  27.4 us (4%)
  other arithmetic  21.3 us (3%)
  loops' own time  20.8 us (3%)
  between operations  14 us (2%)
    reduce_scatter x1, waiting for transfers between devices, on_device(): lax.psum_scatter(lax.optimization_barrier(partial_out).astype(jnp.float32...  185 us
    all_gather x1, blocking collectives, on_device(): shard_rows = lax.all_gather(q_latent, 'tp', axis=0, tiled=True)  157 us
    all_to_all x1, waiting for transfers between devices, on_device(): lax.all_to_all(partial_out.reshape(sources, item_count, feature_width), (...  84.1 us
    another operation x1, loops' own time, on_device(): lax.scan(key_step, start_state, jnp.arange(shard_count // grouping, dtype...  20.2 us
    dot_general x1, matrix products, on_device(): jnp.dot(hidden, down_weight, preferred_element_type=jnp.float32)  19.1 us
    dynamic_slice x32, local copies, waits for them, and re-layouts, on_device(): lax.scan(key_step, start_state, jnp.arange(shard_count // grouping, dtype...  17.9 us
    all_gather x1, waiting for transfers between devices, on_device(): latents = lax.all_gather(kv_latent, ('ep', 'tp'), axis=0, tiled=True)  17 us
    all_to_all x1, starting transfers between devices, on_device(): lax.all_to_all(partial_out.reshape(sources, item_count, feature_width), (...  15.1 us
  transfers between devices with their start and end apart: 5, of which 4 were waited for; matrix products, arithmetic and copies ran while one was open for 17% of the time, Pallas kernels for 0%

commit v1 on v0

--- a/solution.py
+++ b/solution.py
@@ -63,7 +63,10 @@
     group_start = lax.axis_index("ep") * group_rows
     heads_here = w_key.shape[1] // NOPE
     score_scale = (NOPE + ROPE) ** (-0.5)
-    shard_rows = lax.all_gather(q_latent, "tp", axis=0, tiled=True)
+    size = lax.axis_size("tp")
+    blocks = jnp.stack([q_latent for _ in range(size)])
+    blocks = lax.all_to_all(blocks, "tp", split_axis=0, concat_axis=0)
+    shard_rows = jnp.concatenate(blocks, axis=0)
     row_count = shard_rows.shape[0]
     positions = group_start + jnp.arange(row_count, dtype=jnp.int32)
     cosine, sine_table = tables(positions)

time: 616 us -> 690 us (1.12)
  waiting for transfers between devices: 289 us -> 519 us
  blocking collectives: 157 us -> 0 us
    all_gather x1 -> x0, blocking collectives: 157 us -> none  [on_device(): shard_rows = lax.all_gather(q_latent, 'tp', axis=0, tiled=True)]
    all_to_all x1, waiting for transfers between devices: 1.2 us -> 157 us  [on_device(): lax.all_to_all(copies, ('ep', 'tp'), split_axis=0, concat_axis=0, tiled=T...]
    reduce_scatter x1, waiting for transfers between devices: 185 us -> 258 us  [on_device(): lax.psum_scatter(lax.optimization_barrier(partial_out).astype(jnp.float32...]
    all_gather x1, waiting for transfers between devices: 17 us -> 68.3 us  [on_device(): latents = lax.all_gather(kv_latent, ('ep', 'tp'), axis=0, tiled=True)]
    all_to_all x1, waiting for transfers between devices: 84.1 us -> 34.6 us  [on_device(): lax.all_to_all(partial_out.reshape(sources, item_count, feature_width), (...]
  transfers between devices with their start and end apart: 5 -> 6, of which waited for: 4 -> 4; matrix products, arithmetic and copies ran while one was open for 17% -> 15% of each run, Pallas kernels for 0% -> 0%
where the time goes in v1:
time: 690 us; the launch traced here: 684 us
  waiting for transfers between devices  519 us (75%)
  matrix products  52.3 us (8%)
  local copies, waits for them, and re-layouts  29.6 us (4%)
  starting transfers between devices  26.9 us (4%)
  other arithmetic  21.7 us (3%)
  loops' own time  20.8 us (3%)
  between operations  14 us (2%)
    reduce_scatter x1, waiting for transfers between devices, on_device(): lax.psum_scatter(lax.optimization_barrier(partial_out).astype(jnp.float32...  258 us
    all_to_all x1, waiting for transfers between devices, on_device(): lax.all_to_all(copies, ('ep', 'tp'), split_axis=0, concat_axis=0, tiled=T...  157 us
    all_gather x1, waiting for transfers between devices, on_device(): latents = lax.all_gather(kv_latent, ('ep', 'tp'), axis=0, tiled=True)  68.3 us
    all_to_all x1, waiting for transfers between devices, on_device(): lax.all_to_all(partial_out.reshape(sources, item_count, feature_width), (...  34.6 us
    another operation x1, loops' own time, on_device(): lax.scan(key_step, start_state, jnp.arange(shard_count // grouping, dtype...  20.1 us
    dot_general x1, matrix products, on_device(): jnp.dot(hidden, down_weight, preferred_element_type=jnp.float32)  18.8 us
    dynamic_slice x32, local copies, waits for them, and re-layouts, on_device(): lax.scan(key_step, start_state, jnp.arange(shard_count // grouping, dtype...  17.8 us
  transfers between devices with their start and end apart: 6, of which 4 were waited for; matrix products, arithmetic and copies ran while one was open for 15% of the time, Pallas kernels for 0%

profile of v1, /device:TPU:1, one launch (start us, length us, event | category | flops | bytes accessed | tf_op | source)
XLA Modules:
  0.0 684.0 jit_solution(611457448076789501)
XLA Ops:
  7.2 0.7 all-gather.5.cloned.1.call-update
  7.9 1.7 stack.2
  9.7 4.8 all-to-all-start
  14.5 0.7 all-gather.3.cloned.1.call-update
  15.2 0.8 copy.37
  16.2 1.2 reduce-window.6
  18.0 0.7 multiply_add_fusion.1
  18.7 1.2 fusion.47
  19.9 3.9 convolution_convert_fusion.3
  23.8 8.2 %broadcast_in_dim.42 = bf16[32,4,24,2048]{3,2,1,0:T(8,128)(2,1)} broadcast(bf16[32,24,2048]{2,1,0:T(8,128)(2,1)} %bitcast.110), dimensions={0,2,3} | broadcast | bytes 15728640 | tf_op jit(solution)/shard_map/broadcast_in_dim | solution.py:180
  32.0 11.9 %all-to-all-start.1 = ((bf16[128,24,2048]{2,1,0:T(8,128)(2,1)}), bf16[128,24,2048]{2,1,0:T(8,128)(2,1)}, u32[]{:S(2)}, u32[]{:S(2)}) async-start(bf16[128,24,2048]{2,1,0:T(8,128)(2,1)} %bitcast.106), calls=%async_computation.2 | async-start | bytes 25165824 | tf_op jit(solution)/shard_map/all_to_all | solution.py:184
  45.6 156.7 %all-to-all-done.1 = bf16[128,24,2048]{2,1,0:T(8,128)(2,1)} async-done(((bf16[128,24,2048]{2,1,0:T(8,128)(2,1)}), bf16[128,24,2048]{2,1,0:T(8,128)(2,1)}, u32[]{:S(2)}, u32[]{:S(2)}) %all-to-all-start.1) | async-done | bytes 12582944 | tf_op jit(solution)/shard_map/all_to_all | solution.py:184
  202.3 10.0 %fusion.53 = f32[3072,256]{1,0:T(8,128)} fusion(bf16[3072,2048]{1,0:T(8,128)(2,1)} %bitcast.22, bf16[1,2048,256]{2,1,0:T(8,128)(2,1)} %param.35), kind=kOutput, calls=%fused_computation.85 | convolution fusion | flops 3221225472 | bytes 16777216 | tf_op jit(solution)/shard_map/dot_general | solution.py:187
  212.3 18.8 %convolution_convert_fusion.2 = bf16[3072,2048]{1,0:T(8,128)(2,1)} fusion(bf16[3072,2048]{1,0:T(8,128)(2,1)} %bitcast.22, f32[3072,256]{1,0:T(8,128)} %fusion.53, bf16[1,256,2048]{2,1,0:T(8,128)(2,1)S(1)} %copy-done, bf16[1,2048,256]{2,1,0:T(8,128)(2,1)S(1)} %copy-done.11), kind=kOutput, calls=%fused_computation.63 | convolution fusion | flops 6453460992 | bytes 30408704 | tf_op jit(solution)/shard_map/dot_general | solution.py:190
  231.1 9.9 %all-to-all-start.2 = ((bf16[128,24,2048]{2,1,0:T(8,128)(2,1)}), bf16[128,24,2048]{2,1,0:T(8,128)(2,1)}, u32[]{:S(2)}, u32[]{:S(2)}) async-start(bf16[128,24,2048]{2,1,0:T(8,128)(2,1)} %bitcast.109), calls=%async_computation.3 | async-start | bytes 25165824 | tf_op jit(solution)/shard_map/all_to_all | solution.py:193
  241.3 68.3 %all-gather.3.cloned.1.call-done = bf16[16384,256]{1,0:T(8,128)(2,1)} async-done(((bf16[128,256]{1,0:T(8,128)(2,1)}), bf16[16384,256]{1,0:T(8,128)(2,1)}) %all-gather.3.cloned.1.call-update) | async-done | bytes 8388624 | tf_op jit(solution)/shard_map/all_gather | solution.py:90
  309.7 57.2 %while.17 = (s32[]{:T(128)}, f32[4,512]{1,0:T(4,128)S(1)}, f32[4,512]{1,0:T(4,128)S(1)}, f32[4,512,64]{1,2,0:T(8,128)S(1)}, s32[32]{0:T(128)S(1)}, /*index=5*/s3...) while((s32[]{:T(128)}, f32[4,512]{1,0:T(4,128)S(1)}, ...), condition=%wide.region_7.8_spmd.clone, body=%wide.region_1.7_spmd.clone.sunk | while | flops 482656832 | bytes 25966364 | solution.py:137
  309.7 0.6 dynamic_slice.20
  310.9 9.0 %conditional.3 = ((f32[4,512]{1,0:T(4,128)S(1)}, f32[4,512]{1,0:T(4,128)S(1)}, f32[4,512,64]{1,2,0:T(8,128)S(1)})) conditional(s32[]{:T(128)} %convert_element_type.202, (f32[4,512]{1,0:T(4,128)S(1)}, f32[4,512]{1,0:T(4,128)S(1)}, f32[4,512,64]{1,2,0:T(8,128)S(1)}) %tuple.60, (s32[]{:T(128)}, s32[512]{0:T(512)S(1)}, bf16[16384,256]{1,0:T(8,128)(2,1)}, ...), branch_computations={%region_2.2_spmd, %region_3.6_spmd} | conditional | flops 482649632 | bytes 25957090 | solution.py:132
  311.0 1.1 fusion.14
  312.1 1.3 convolution_convert_fusion.1
  313.4 0.8 fusion.85
  314.2 0.9 dynamic-slice_convert_fusion
  315.5 1.2 fusion.84
  316.8 0.8 fusion.5
  317.6 1.3 convolution_convert_fusion
  318.9 1.0 fusion.11
  319.9 0.6 dynamic_slice.20
  321.1 9.0 %conditional.3 = ((f32[4,512]{1,0:T(4,128)S(1)}, f32[4,512]{1,0:T(4,128)S(1)}, f32[4,512,64]{1,2,0:T(8,128)S(1)})) conditional(s32[]{:T(128)} %convert_element_type.202, (f32[4,512]{1,0:T(4,128)S(1)}, f32[4,512]{1,0:T(4,128)S(1)}, f32[4,512,64]{1,2,0:T(8,128)S(1)}) %tuple.60, (s32[]{:T(128)}, s32[512]{0:T(512)S(1)}, bf16[16384,256]{1,0:T(8,128)(2,1)}, ...), branch_computations={%region_2.2_spmd, %region_3.6_spmd} | conditional | flops 482649632 | bytes 25957090 | solution.py:132
  321.1 1.1 fusion.14
  322.3 1.3 convolution_convert_fusion.1
  323.6 0.8 fusion.85
  324.3 0.9 dynamic-slice_convert_fusion
  325.7 1.2 fusion.84
  326.9 0.8 fusion.5
  327.7 1.3 convolution_convert_fusion
  329.1 1.0 fusion.11
  330.1 0.6 dynamic_slice.20
  346.0 0.6 dynamic_slice.20
  352.2 0.6 dynamic_slice.20
  367.0 2.1 convolution_convert_fusion.4
  369.1 34.6 %all-to-all-done.2 = bf16[128,24,2048]{2,1,0:T(8,128)(2,1)} async-done(((bf16[128,24,2048]{2,1,0:T(8,128)(2,1)}), bf16[128,24,2048]{2,1,0:T(8,128)(2,1)}, u32[]{:S(2)}, u32[]{:S(2)}) %all-to-all-start.2) | async-done | bytes 12582944 | tf_op jit(solution)/shard_map/all_to_all | solution.py:193
  403.7 10.4 %bitcast_reduce_fusion = bf16[32,24,2048]{2,1,0:T(8,128)(2,1)} fusion(bf16[128,24,2048]{2,1,0:T(8,128)(2,1)} %all-to-all-done.2), kind=kLoop, calls=%fused_computation.62 | loop fusion | flops 4718592 | bytes 15728640 | tf_op jit(solution)/shard_map/reduce_sum | solution.py:202
  414.0 2.7 convolution_multiply_fusion.2
  416.9 0.6 convolution_multiply_fusion.3
  417.5 0.7 convolution_multiply_fusion.1
  418.2 1.6 fusion.45
  419.8 257.6 %reduce-scatter.2.cloned.1.call-done = bf16[128,2048]{1,0:T(8,128)(2,1)} async-done(((bf16[512,2048]{1,0:T(8,128)(2,1)}), bf16[128,2048]{1,0:T(8,128)(2,1)}) %reduce-scatter.2.cloned.1.call-update) | async-done | bytes 524304 | tf_op jit(solution)/shard_map/reduce_scatter | solution.py:151
  (262 shorter events, 20.3 us)
Async XLA Ops:
  7.2 205.1 %copy-start = (bf16[1,256,2048]{2,1,0:T(8,128)(2,1)S(1)}, bf16[1,256,2048]{2,1,0:T(8,128)(2,1)}, u32[]{:S(2)}) copy-start(bf16[1,256,2048]{2,1,0:T(8,128)(2,1)} %param.37) | copy-start | bytes 3145732
  7.2 234.1 %all-gather.5.cloned.1.call-start = ((), (), s32[]{:S(2)}) async-start(), calls=%async_computation.5 | async-start | bytes 1056768 | tf_op jit(solution)/shard_map/all_gather | solution.py:91
  9.7 14.2 %all-to-all-start = ((bf16[4,128,512]{2,1,0:T(8,128)(2,1)}), bf16[4,128,512]{2,1,0:T(8,128)(2,1)S(1)}, u32[]{:S(2)}, u32[]{:S(2)}) async-start(bf16[4,128,512]{2,1,0:T(8,128)(2,1)} %stack.2), calls=%async_computation | async-start | bytes 1048576 | tf_op jit(solution)/shard_map/all_to_all | solution.py:68
  14.5 295.1 %all-gather.3.cloned.1.call-start = ((), (), s32[]{:S(2)}) async-start(), calls=%async_computation.4 | async-start | bytes 8454144 | tf_op jit(solution)/shard_map/all_gather | solution.py:90
  32.0 11.9 %copy-start.7 = (bf16[512,128]{1,0:T(8,128)(2,1)S(1)}, bf16[512,128]{1,0:T(8,128)(2,1)}, u32[]{:S(2)}) copy-start(bf16[512,128]{1,0:T(8,128)(2,1)} %param.27) | copy-start | bytes 393220
  32.0 12.4 %copy-start.9 = (f32[512]{0:T(512)S(1)}, f32[512]{0:T(512)}, u32[]{:S(2)}) copy-start(f32[512]{0:T(512)} %param.24) | copy-start | bytes 6148
  32.0 170.3 %all-to-all-start.1 = ((bf16[128,24,2048]{2,1,0:T(8,128)(2,1)}), bf16[128,24,2048]{2,1,0:T(8,128)(2,1)}, u32[]{:S(2)}, u32[]{:S(2)}) async-start(bf16[128,24,2048]{2,1,0:T(8,128)(2,1)} %bitcast.106), calls=%async_computation.2 | async-start | bytes 25165824 | tf_op jit(solution)/shard_map/all_to_all | solution.py:184
  43.9 1.3 copy-start.6
  202.3 10.0 %copy-start.11 = (bf16[1,2048,256]{2,1,0:T(8,128)(2,1)S(1)}, bf16[1,2048,256]{2,1,0:T(8,128)(2,1)}, u32[]{:S(2)}) copy-start(bf16[1,2048,256]{2,1,0:T(8,128)(2,1)} %param.36) | copy-start | bytes 3145732
  231.1 78.6 %copy-start.3 = (bf16[256,256]{1,0:T(8,128)(2,1)S(1)}, bf16[256,256]{1,0:T(8,128)(2,1)}, u32[]{:S(2)}) copy-start(bf16[256,256]{1,0:T(8,128)(2,1)} %param.28) | copy-start | bytes 393220
  231.1 78.6 %copy-start.4 = (bf16[256,256]{1,0:T(8,128)(2,1)S(1)}, bf16[256,256]{1,0:T(8,128)(2,1)}, u32[]{:S(2)}) copy-start(bf16[256,256]{1,0:T(8,128)(2,1)} %param.29) | copy-start | bytes 393220
  231.1 78.6 %copy-start.8 = (f32[256]{0:T(256)S(1)}, f32[256]{0:T(256)}, u32[]{:S(2)}) copy-start(f32[256]{0:T(256)} %param.25) | copy-start | bytes 3076
  231.1 172.6 %all-to-all-start.2 = ((bf16[128,24,2048]{2,1,0:T(8,128)(2,1)}), bf16[128,24,2048]{2,1,0:T(8,128)(2,1)}, u32[]{:S(2)}, u32[]{:S(2)}) async-start(bf16[128,24,2048]{2,1,0:T(8,128)(2,1)} %bitcast.109), calls=%async_computation.3 | async-start | bytes 25165824 | tf_op jit(solution)/shard_map/all_to_all | solution.py:193
  241.0 436.5 %reduce-scatter.2.cloned.1.call-start = ((), (), s32[]{:S(2)}) async-start(), calls=%async_computation.6 | async-start | bytes 2621440 | tf_op jit(solution)/shard_map/reduce_scatter | solution.py:151
  309.7 57.2 %copy-start.5 = (bf16[256,2048]{1,0:T(8,128)(2,1)S(1)}, bf16[256,2048]{1,0:T(8,128)(2,1)}, u32[]{:S(2)}) copy-start(bf16[256,2048]{1,0:T(8,128)(2,1)} %param.30) | copy-start | bytes 3145732
  366.9 2.2 copy-start.10
  414.0 2.8 copy-start.2
  417.5 259.9 %copy-start.1 = (bf16[1,256,2048]{2,1,0:T(8,128)(2,1)S(1)}, bf16[1,256,2048]{2,1,0:T(8,128)(2,1)}, u32[]{:S(2)}) copy-start(bf16[1,256,2048]{2,1,0:T(8,128)(2,1)} %param.37) | copy-start | bytes 3145732
Sparse Core Ops, SparseCore 0:
  10.8 147.3 all-gather.4
  161.3 148.2 all-gather.2
  369.2 308.1 reduce-scatter.1
